TPU v7x, 32 devices: a whole 2x2x4 slice. The times are simulated.
32 devices in a mesh: rep: 2 (over y), fs: 4 (over z), tp: 4 (over x, core).
Axes of the slice: x: 2, y: 2, z: 4, core: 2. Of those that a mesh axis runs over, the one named last changes fastest.
Arguments:
- stream: bfloat16 [4096, 2048], P(('rep', 'fs', 'tp')), may hold values from -6 to 6
- gain_before: float32 [2048], replicated, may hold values from 0.1 to 1.9
- gain_after: float32 [2048], replicated, may hold values from 0.1 to 1.9
- proj_gate: bfloat16 [2048, 3584], P('fs', 'tp'), may hold values from -0.125 to 0.125
- proj_lift: bfloat16 [2048, 3584], P('fs', 'tp'), may hold values from -0.125 to 0.125
- proj_down: bfloat16 [3584, 2048], P('tp', 'fs'), may hold values from -0.09375 to 0.09375
- mixer_gain: float32 [2048], replicated, may hold values from 0.1 to 1.9
- mixer_u: bfloat16 [2048, 2048], P('fs', 'tp'), may hold values from -0.125 to 0.125
- mixer_v: bfloat16 [2048, 2048], P('fs', 'tp'), may hold values from -1 to 1
- layer_gain: float32 [2048], P('tp'), may hold values from 0.1 to 1.9
- layer_shift: float32 [2048], P('tp'), may hold values from -3 to 3
- spatial: bfloat16 [16, 128, 128], P('tp'), may hold values from -0.5 to 0.5
- spatial_shift: float32 [16, 128], P('tp'), may hold values from 0.2 to 2
- mixer_down: bfloat16 [2048, 2048], P('tp', 'fs'), may hold values from -0.125 to 0.125
Outputs:
- result: bfloat16 [4096, 2048], P(('rep', 'fs', 'tp'))
All inputs are finite; a program needn't handle non-finite values.
Results may differ from a plain program's by a relative error of at most 0.017.
Values may be sent and summed in bfloat16 or wider, within the bound.
A program may use at most 128 MiB of HBM per device.

v0:
```python
import functools

import jax
import jax.numpy as jnp
from jax import lax
from jax.experimental import pallas as pl
from jax.experimental.pallas import tpu as pltpu
from jax.sharding import PartitionSpec as P

SPAN = 128

norm_epsilon = 1e-06
layer_epsilon = 1e-05

MESH = pl.DeviceIdType.MESH
GATE, LIFT, DOWN, MIX_U, MIX_V, MIX_DOWN = range(6)
CUTS = 2
AHEAD = 1


def norm_rows(widened, scale_gain):
    factor = lax.rsqrt(jnp.mean(widened * widened, axis=1, keepdims=True) + norm_epsilon)
    return (widened * factor * scale_gain).astype(jnp.bfloat16)


def layer_kernel(
    n_rep,
    n_fs,
    n_tp,
    stream,
    gain_before,
    gain_after,
    mixer_gain,
    layer_gain,
    layer_shift,
    spatial,
    spatial_shift,
    proj_gate,
    proj_lift,
    proj_down,
    mixer_u,
    mixer_v,
    mixer_down,
    out,
    gate_all,
    lift_all,
    down_all,
    u_all,
    v_all,
    mix_down_all,
    rows_all,
    to_sibling,
    from_sibling,
    to_chip,
    from_chip,
    partial_all,
    gate_vals,
    hidden,
    u_vals,
    lifted,
    gated,
    mom_own,
    mom_in,
    square,
    resid,
    local_sem,
    z_send,
    z_send_left,
    z_recv,
    y_send,
    y_recv,
    ag_sem,
    agf_sem,
    sib_sem,
    chip_sem,
    mom_sem,
):
    rep, fs, tp = lax.axis_index("rep"), lax.axis_index("fs"), lax.axis_index("tp")
    chip, core = tp // 2, lax.rem(tp, 2)
    n_chip = n_tp // 2
    block, width = stream.shape
    pair = 2 * block
    shards = (proj_gate, proj_lift, proj_down, mixer_u, mixer_v, mixer_down)
    full = (gate_all, lift_all, down_all, u_all, v_all, mix_down_all)
    mine = pl.ds(pl.multiple_of(core * block, block), block)
    theirs = pl.ds(pl.multiple_of((1 - core) * block, block), block)
    sibling = chip * 2 + (1 - core)

    def at(r, f, t):
        return (r, f, t)

    barrier = pltpu.get_barrier_semaphore()

    @pl.when(fs > 0)
    def _():
        pl.semaphore_signal(barrier, inc=1, device_id=at(rep, fs - 1, tp), device_id_type=MESH)

    @pl.when(fs < n_fs - 1)
    def _():
        pl.semaphore_signal(barrier, inc=1, device_id=at(rep, fs + 1, tp), device_id_type=MESH)

    for k in range(1, n_rep):
        pl.semaphore_signal(
            barrier, inc=1, device_id=at(lax.rem(rep + k, n_rep), fs, tp), device_id_type=MESH
        )
    for k in range(1, n_tp):
        pl.semaphore_signal(
            barrier, inc=1, device_id=at(rep, fs, lax.rem(tp + k, n_tp)), device_id_type=MESH
        )

    locals_ = [
        pltpu.make_async_copy(shards[w], full[w].at[fs], local_sem.at[w]) for w in range(6)
    ]
    for copy in locals_:
        copy.start()

    line_peers = jnp.minimum(fs, 1) + jnp.minimum(n_fs - 1 - fs, 1)
    pl.semaphore_wait(barrier, n_rep - 1 + n_tp - 1 + line_peers)

    items = 6 * CUTS

    def piece(i, owner, part):
        w, cut = i // CUTS, i % CUTS
        rows = full[w].shape[1] // (n_rep * CUTS)
        first_row = pl.multiple_of((part * CUTS + cut) * rows, rows)
        return full[w].at[owner, pl.ds(first_row, rows)]

    def z_copy(i, owner, step):
        ref = piece(i, owner, rep)
        sem = z_send.at[i, owner] if step > 0 else z_send_left.at[i, owner]
        return pltpu.make_async_remote_copy(
            src_ref=ref, dst_ref=ref, send_sem=sem, recv_sem=z_recv.at[i, owner],
            device_id=at(rep, fs + step, tp), device_id_type=MESH,
        )

    def y_copy(i, owner, k):
        ref = piece(i, owner, rep)
        return pltpu.make_async_remote_copy(
            src_ref=ref, dst_ref=ref, send_sem=y_send.at[i, k - 1, owner],
            recv_sem=y_recv.at[i, k - 1, owner],
            device_id=at(lax.rem(rep + k, n_rep), fs, tp), device_id_type=MESH,
        )

    def own(i):
        if i % CUTS == 0:
            locals_[i // CUTS].wait()

        @pl.when(fs < n_fs - 1)
        def _():
            z_copy(i, fs, 1).start()

        @pl.when(fs > 0)
        def _():
            z_copy(i, fs, -1).start()

    def serve(i):
        if i + AHEAD < items:
            own(i + AHEAD)

        def hop(h, carry):
            @pl.when(fs >= h)
            def _():
                z_copy(i, fs - h, 1).wait_recv()

                @pl.when(fs < n_fs - 1)
                def _():
                    z_copy(i, fs - h, 1).start()

                for k in range(1, n_rep):
                    y_copy(i, fs - h, k).start()

            @pl.when(fs + h < n_fs)
            def _():
                z_copy(i, fs + h, -1).wait_recv()

                @pl.when(fs > 0)
                def _():
                    z_copy(i, fs + h, -1).start()

                for k in range(1, n_rep):
                    y_copy(i, fs + h, k).start()

            return carry

        lax.fori_loop(1, n_fs, hop, 0)

    def pump(w):
        for cut in range(CUTS):
            serve(w * CUTS + cut)

    def arrived(w):
        def one(h, carry):
            owner = lax.rem(fs + h, n_fs)
            for cut in range(CUTS):
                i = w * CUTS + cut
                for k in range(1, n_rep):
                    source = lax.rem(rep + n_rep - k, n_rep)
                    ref = piece(i, owner, source)
                    pltpu.make_async_remote_copy(
                        src_ref=ref, dst_ref=ref, send_sem=y_send.at[i, k - 1, owner],
                        recv_sem=y_recv.at[i, k - 1, owner],
                        device_id=at(source, fs, tp), device_id_type=MESH,
                    ).wait_recv()
            return carry

        lax.fori_loop(1, n_fs, one, 0)

    def sends_done():
        def one(owner, carry):
            for i in range(items):
                @pl.when((owner <= fs) & (fs < n_fs - 1))
                def _():
                    z_copy(i, owner, 1).wait_send()

                @pl.when((owner >= fs) & (fs > 0))
                def _():
                    z_copy(i, owner, -1).wait_send()

                @pl.when(owner != fs)
                def _():
                    for k in range(1, n_rep):
                        y_copy(i, owner, k).wait_send()

            return carry

        lax.fori_loop(0, n_fs, one, 0)

    def other_chip(k):
        return lax.rem(chip + k, n_chip)

    def source_chip(k):
        return lax.rem(chip + n_chip - k, n_chip)

    def tp_copy(src, dst, send, recv, target):
        return pltpu.make_async_remote_copy(
            src_ref=src, dst_ref=dst, send_sem=send, recv_sem=recv,
            device_id=at(rep, fs, target), device_id_type=MESH,
        )

    def gather_copy(phase, k):
        ref = rows_all.at[phase, chip, mine]
        target = other_chip(k) * 2 + core
        return tp_copy(ref, ref, ag_sem.at[0, phase, k], ag_sem.at[1, phase, k], target)

    def pass_copy(phase, k):
        ref = rows_all.at[phase, source_chip(k), mine]
        return tp_copy(ref, ref, agf_sem.at[0, phase, k], agf_sem.at[1, phase, k], sibling)

    def gather_start(phase, normed):
        rows_all[phase, chip, mine] = normed
        for k in range(1, n_chip):
            gather_copy(phase, k).start()
        pass_copy(phase, 0).start()

    def gather_pass(phase):
        for k in range(1, n_chip):
            gather_copy(phase, k).wait_recv()
            pass_copy(phase, k).start()

    def gather_end(phase):
        for k in range(1, n_chip):
            gather_copy(phase, k).wait_send()
        for k in range(n_chip):
            pass_copy(phase, k).wait_send()

    def each_pair(compute):
        def one(p, carry):
            compute(p)
            return carry

        lax.fori_loop(0, n_chip, one, 0)

    def sib_copy(phase, p):
        return tp_copy(
            to_sibling.at[phase, p], from_sibling.at[phase, p],
            sib_sem.at[0, phase, p], sib_sem.at[1, phase, p], sibling,
        )

    def chip_copy(phase, k):
        return tp_copy(
            to_chip.at[phase, k - 1], from_chip.at[phase, k - 1],
            chip_sem.at[0, phase, k], chip_sem.at[1, phase, k], other_chip(k) * 2 + core,
        )

    def reduce(phase, left, w, meanwhile=None):
        cols = full[w].shape[2]

        def product(p):
            def one(f, carry):
                partial_all[f] = jnp.dot(left[p], full[w][f], preferred_element_type=jnp.float32)
                return carry

            lax.fori_loop(0, n_fs, one, 0)
            for f in range(n_fs):
                to_sibling[phase, p, :, f * cols : (f + 1) * cols] = partial_all[f, theirs].astype(
                    jnp.bfloat16
                )
            sib_copy(phase, p).start()

        def joined(p):
            sib_copy(phase, p).wait_recv()
            held = jnp.concatenate([partial_all[f, mine] for f in range(n_fs)], axis=1)
            return held + from_sibling[phase, p].astype(jnp.float32)

        def away(k, carry):
            p = other_chip(k)
            product(p)
            to_chip[phase, k - 1] = joined(p).astype(jnp.bfloat16)
            chip_copy(phase, k).start()
            return carry

        lax.fori_loop(1, n_chip, away, 0)
        product(chip)
        total = joined(chip)
        if meanwhile is not None:
            meanwhile()
        for k in range(1, n_chip):
            chip_copy(phase, k).wait_recv()
            total = total + from_chip[phase, k - 1].astype(jnp.float32)
        for k in range(1, n_chip):
            chip_copy(phase, k).wait_send()
        for p in range(n_chip):
            sib_copy(phase, p).wait_send()
        return total

    def project(phase, p, w):
        rows = full[w].shape[1]
        total = None
        for f in range(n_fs):
            term = jnp.dot(
                rows_all[phase, p, :, f * rows : (f + 1) * rows], full[w][f],
                preferred_element_type=jnp.float32,
            )
            total = term if total is None else total + term
        return total

    def gate_pair(phase):
        def compute(p):
            gate_vals[p] = project(phase, p, GATE)

        return compute

    def lift_pair(phase):
        def compute(p):
            hidden[p] = (jax.nn.silu(gate_vals[p]) * project(phase, p, LIFT)).astype(jnp.bfloat16)

        return compute

    gather_start(0, norm_rows(stream[...].astype(jnp.float32), gain_before[...]))
    for i in range(AHEAD):
        own(i)
    pass_copy(0, 0).wait_recv()
    pump(GATE)
    gather_pass(0)
    for k in range(1, n_chip):
        pass_copy(0, k).wait_recv()
    arrived(GATE)
    each_pair(gate_pair(0))
    pump(LIFT)
    arrived(LIFT)
    each_pair(lift_pair(0))
    pump(DOWN)
    arrived(DOWN)
    total = reduce(0, hidden, DOWN, lambda: pump(MIX_U))
    first = (stream[...].astype(jnp.float32) + 0.5 * total).astype(jnp.bfloat16)
    resid[...] = first
    gather_end(0)

    gather_start(1, norm_rows(first.astype(jnp.float32), mixer_gain[...]))
    pump(MIX_V)
    pass_copy(1, 0).wait_recv()
    gather_pass(1)
    for k in range(1, n_chip):
        pass_copy(1, k).wait_recv()
    arrived(MIX_U)

    def u_pair(p):
        u_vals[p] = jax.nn.gelu(project(1, p, MIX_U))

    each_pair(u_pair)
    arrived(MIX_V)

    def v_pair(p):
        values = jax.nn.gelu(project(1, p, MIX_V))
        lifted[p] = values
        sums = jnp.sum(values, axis=1, keepdims=True)
        squares = jnp.sum(values * values, axis=1, keepdims=True)
        lane = lax.broadcasted_iota(jnp.int32, (pair, 128), 1)
        both = jnp.where(lane == 0, sums, jnp.where(lane == 1, squares, 0.0))
        mom_own[p] = both.T[:8]

    each_pair(v_pair)

    def mom_copy(k):
        return tp_copy(
            mom_own, mom_in.at[k - 1], mom_sem.at[0, k], mom_sem.at[1, k], lax.rem(tp + k, n_tp)
        )

    for k in range(1, n_tp):
        mom_copy(k).start()
    pump(MIX_DOWN)
    square[...] = jnp.zeros_like(square)
    groups = spatial.shape[0]
    square[0:groups, :] = spatial_shift[...]
    shift_columns = square[...].T
    for k in range(1, n_tp):
        mom_copy(k).wait_recv()
    channels = lifted.shape[2]
    group_dim = channels // groups
    all_channels = channels * n_tp

    def mix_pair(p):
        moments = mom_own[p]
        for k in range(1, n_tp):
            moments = moments + mom_in[k - 1, p]
        moments = moments * (1.0 / all_channels)
        columns = jnp.concatenate([moments, jnp.zeros((120, pair), jnp.float32)], axis=0).T
        centre = columns[:, 0:1]
        spread = columns[:, 1:2] - centre * centre
        normed_v = (
            (lifted[p] - centre) * lax.rsqrt(spread + layer_epsilon) * layer_gain[...]
            + layer_shift[...]
        ).astype(jnp.bfloat16)
        row = lax.broadcasted_iota(jnp.int32, (SPAN, SPAN), 0)
        col = lax.broadcasted_iota(jnp.int32, (SPAN, SPAN), 1)
        for g in range(groups):
            masked = jnp.where(row >= col, spatial[g].astype(jnp.float32), 0.0).astype(
                jnp.bfloat16
            )
            cut = slice(g * group_dim, (g + 1) * group_dim)
            for b in range(pair // SPAN):
                span = slice(b * SPAN, (b + 1) * SPAN)
                mixed = jnp.dot(masked, normed_v[span, cut], preferred_element_type=jnp.float32)
                mixed = mixed + shift_columns[:, g : g + 1]
                gated[p, span, cut] = (u_vals[p, span, cut] * mixed).astype(jnp.bfloat16)

    each_pair(mix_pair)
    for k in range(1, n_tp):
        mom_copy(k).wait_send()
    arrived(MIX_DOWN)
    total = reduce(1, gated, MIX_DOWN)
    second = (resid[...].astype(jnp.float32) + total).astype(jnp.bfloat16)
    resid[...] = second
    gather_end(1)

    gather_start(2, norm_rows(second.astype(jnp.float32), gain_after[...]))
    pass_copy(2, 0).wait_recv()
    gate_pair(2)(chip)
    lift_pair(2)(chip)
    gather_pass(2)
    for k in range(1, n_chip):
        pass_copy(2, k).wait_recv()

    def last_pair(k, carry):
        gate_pair(2)(other_chip(k))
        lift_pair(2)(other_chip(k))
        return carry

    lax.fori_loop(1, n_chip, last_pair, 0)
    total = reduce(2, hidden, DOWN)
    out[...] = (resid[...].astype(jnp.float32) + 0.5 * total).astype(jnp.bfloat16)
    gather_end(2)
    sends_done()


def body(
    n_rep,
    n_fs,
    n_tp,
    stream,
    gain_before,
    gain_after,
    proj_gate,
    proj_lift,
    proj_down,
    mixer_gain,
    mixer_u,
    mixer_v,
    layer_gain,
    layer_shift,
    spatial,
    spatial_shift,
    mixer_down,
):
    block, width = stream.shape
    n_chip = n_tp // 2
    pair = 2 * block
    units = proj_gate.shape[1]
    channels = mixer_u.shape[1]
    bf16, f32 = jnp.bfloat16, jnp.float32
    shards = (proj_gate, proj_lift, proj_down, mixer_u, mixer_v, mixer_down)
    vmem = pl.BlockSpec(memory_space=pltpu.VMEM)
    anywhere = pl.BlockSpec(memory_space=pl.ANY)
    dma = pltpu.SemaphoreType.DMA
    spread_reps = max(n_rep - 1, 1)
    spread_chips = max(n_chip - 1, 1)
    return pl.pallas_call(
        functools.partial(layer_kernel, n_rep, n_fs, n_tp),
        out_shape=jax.ShapeDtypeStruct((block, width), bf16),
        in_specs=[vmem] * 8 + [anywhere] * 6,
        out_specs=vmem,
        scratch_shapes=[pltpu.VMEM((n_fs,) + w.shape, bf16) for w in shards]
        + [
            pltpu.VMEM((3, n_chip, pair, width), bf16),
            pltpu.VMEM((3, n_chip, block, width), bf16),
            pltpu.VMEM((3, n_chip, block, width), bf16),
            pltpu.VMEM((3, spread_chips, block, width), bf16),
            pltpu.VMEM((3, spread_chips, block, width), bf16),
            pltpu.VMEM((n_fs, pair, width // n_fs), f32),
            pltpu.VMEM((n_chip, pair, units), f32),
            pltpu.VMEM((n_chip, pair, units), bf16),
            pltpu.VMEM((n_chip, pair, channels), f32),
            pltpu.VMEM((n_chip, pair, channels), f32),
            pltpu.VMEM((n_chip, pair, channels), bf16),
            pltpu.VMEM((n_chip, 8, pair), f32),
            pltpu.VMEM((max(n_tp - 1, 1), n_chip, 8, pair), f32),
            pltpu.VMEM((128, SPAN), f32),
            pltpu.VMEM((block, width), bf16),
            dma((6,)),
            dma((6 * CUTS, n_fs)),
            dma((6 * CUTS, n_fs)),
            dma((6 * CUTS, n_fs)),
            dma((6 * CUTS, spread_reps, n_fs)),
            dma((6 * CUTS, spread_reps, n_fs)),
            dma((2, 3, n_chip)),
            dma((2, 3, n_chip)),
            dma((2, 3, n_chip)),
            dma((2, 3, n_chip)),
            dma((2, n_tp)),
        ],
        compiler_params=pltpu.CompilerParams(
            collective_id=0, has_side_effects=True, vmem_limit_bytes=60 * 1024 * 1024
        ),
    )(
        stream,
        gain_before.reshape(1, -1),
        gain_after.reshape(1, -1),
        mixer_gain.reshape(1, -1),
        layer_gain.reshape(1, -1),
        layer_shift.reshape(1, -1),
        spatial,
        spatial_shift,
        *shards,
    )


def solution(mesh):
    placed = (
        P(("rep", "fs", "tp"), None),
        P(),
        P(),
        P("fs", "tp"),
        P("fs", "tp"),
        P("tp", "fs"),
        P(),
        P("fs", "tp"),
        P("fs", "tp"),
        P("tp"),
        P("tp"),
        P("tp", None, None),
        P("tp", None),
        P("tp", "fs"),
    )
    sizes = (mesh.shape["rep"], mesh.shape["fs"], mesh.shape["tp"])
    return jax.shard_map(
        functools.partial(body, *sizes),
        mesh=mesh,
        in_specs=placed,
        out_specs=P(("rep", "fs", "tp"), None),
        check_vma=False,
    )
```

profile of v0, /device:TPU:0, one launch (start us, length us, event | category | flops | bytes accessed | tf_op | source)
XLA Modules:
  0.0 228.9 jit_solution(1662691711300817000)
XLA Ops:
  0.0 227.0 %shard_map.136 = bf16[128,2048]{1,0:T(8,128)(2,1)} custom-call(bf16[128,2048]{1,0:T(8,128)(2,1)} %stream.1, f32[1,2048]{1,0:T(1,128)} %bitcast.5, f32[1,2048]{1,0:T(1,128)} %bitcast.6, f32[1,2048]{1,0:T(1,128)} %bitcast.7, f32[1,512]{1,0:T(1,128)} %bitcast.8, f32[1,512]{1,0:T(1,128)} %bitcast.9, bf16[4,128,128]{2,1,0:T(8,128)(2,1)} %spatial.1, ...), custom_call_target="tpu_custom_call" | custom-call | tf_op jit(solution)/shard_map/pallas_call | solution.py:497
  227.0 1.9 copy.16
where the time goes:
time: 229 us
  Pallas kernels  227 us (99%)
    pallas_call x1, Pallas kernels, body(): pl.pallas_call(functools.partial(layer_kernel, n_rep, n_fs, n_tp), out_sh...  227 us

commit v1 on v0

v1 whole, which is shorter than its diff:
```python
import functools

import jax
import jax.numpy as jnp
from jax import lax
from jax.experimental import pallas as pl
from jax.experimental.pallas import tpu as pltpu
from jax.sharding import PartitionSpec as P

SPAN = 128

norm_epsilon = 1e-06
layer_epsilon = 1e-05

MESH = pl.DeviceIdType.MESH
GATE, LIFT, DOWN, MIX_U, MIX_V, MIX_DOWN = range(6)
CUTS = 2
AHEAD = 3
NEAR = 1
HALVES = 2
MIXERS = (MIX_U, MIX_V, MIX_DOWN)
BY_ROWS = (GATE, LIFT, MIX_U, MIX_V)


def norm_rows(widened, scale_gain):
    factor = lax.rsqrt(jnp.mean(widened * widened, axis=1, keepdims=True) + norm_epsilon)
    return (widened * factor * scale_gain).astype(jnp.bfloat16)


def layer_kernel(
    n_rep,
    n_fs,
    n_tp,
    stream,
    gain_before,
    gain_after,
    mixer_gain,
    layer_gain,
    layer_shift,
    spatial,
    spatial_shift,
    proj_gate,
    proj_lift,
    proj_down,
    mixer_u,
    mixer_v,
    mixer_down,
    out,
    gate_all,
    lift_all,
    down_all,
    u_all,
    v_all,
    mix_down_all,
    rows_all,
    to_sibling,
    from_sibling,
    to_chip,
    from_chip,
    part,
    hold,
    gate_vals,
    hidden,
    u_vals,
    lifted,
    gated,
    rows_last,
    hidden_last,
    part_half,
    masked,
    mom_own,
    mom_in,
    square,
    resid,
    local_sem,
    z_send,
    z_recv,
    y_send,
    y_recv,
    ag_sem,
    agf_sem,
    sib_sem,
    chip_sem,
    mom_sem,
    token_sem,
    second_sem,
    agl_sem,
    last_sem,
):
    rep, fs, tp = lax.axis_index("rep"), lax.axis_index("fs"), lax.axis_index("tp")
    chip, core = tp // 2, lax.rem(tp, 2)
    n_chip = n_tp // 2
    block, width = stream.shape
    pair = 2 * block
    cols = width // n_fs
    shards = (proj_gate, proj_lift, proj_down, mixer_u, mixer_v, mixer_down)
    full = (gate_all, lift_all, down_all, u_all, v_all, mix_down_all)
    mine = pl.ds(pl.multiple_of(core * block, block), block)
    theirs = pl.ds(pl.multiple_of((1 - core) * block, block), block)
    sibling = chip * 2 + (1 - core)

    spread = n_fs >= 4
    depth = jnp.minimum(fs, n_fs - 1 - fs)
    side = (2 * fs) // n_fs
    inward = 1 - 2 * side
    if spread:
        low_slot = lax.rem(jnp.minimum(depth, 2) + 2, 3)
        at_end, at_mid = depth == 0, depth == 1
    else:
        low_slot = 1
    busy = low_slot < 2

    def when_busy(run):
        if spread:
            pl.when(busy)(run)
        else:
            run()

    def when_mid(run):
        if spread:
            pl.when(at_mid)(run)

    def when_end(run):
        if spread:
            pl.when(at_end)(run)

    def low_depth(w):
        return 1 if spread and w in MIXERS else 0

    def at(r, f, t):
        return (r, f, t)

    barrier = pltpu.get_barrier_semaphore()

    @pl.when(fs > 0)
    def _():
        pl.semaphore_signal(barrier, inc=1, device_id=at(rep, fs - 1, tp), device_id_type=MESH)

    @pl.when(fs < n_fs - 1)
    def _():
        pl.semaphore_signal(barrier, inc=1, device_id=at(rep, fs + 1, tp), device_id_type=MESH)

    for k in range(1, n_rep):
        pl.semaphore_signal(
            barrier, inc=1, device_id=at(lax.rem(rep + k, n_rep), fs, tp), device_id_type=MESH
        )
    for k in range(1, n_tp):
        pl.semaphore_signal(
            barrier, inc=1, device_id=at(rep, fs, lax.rem(tp + k, n_tp)), device_id_type=MESH
        )

    def depth_of(w):
        return shards[w].shape[0]

    def whole(w, owner):
        if w in BY_ROWS:
            n = depth_of(w)
            return full[w].at[pl.ds(pl.multiple_of(owner * n, n), n)]
        return full[w].at[owner]

    locals_ = [
        pltpu.make_async_copy(shards[w], whole(w, fs), local_sem.at[w]) for w in range(6)
    ]
    for copy in locals_:
        copy.start()

    line_peers = jnp.minimum(fs, 1) + jnp.minimum(n_fs - 1 - fs, 1)
    pl.semaphore_wait(barrier, n_rep - 1 + n_tp - 1 + line_peers)

    items = 6 * CUTS

    def piece(i, owner, part_index):
        w, cut = i // CUTS, i % CUTS
        rows = depth_of(w) // (n_rep * CUTS)
        first_row = (part_index * CUTS + cut) * rows
        if w in BY_ROWS:
            start = pl.multiple_of(owner * depth_of(w) + first_row, rows)
            return full[w].at[pl.ds(start, rows)]
        return full[w].at[owner, pl.ds(pl.multiple_of(first_row, rows), rows)]

    def z_copy(i, owner, out):
        ref = piece(i, owner, rep)
        step = inward if out == 0 else -inward
        return pltpu.make_async_remote_copy(
            src_ref=ref, dst_ref=ref, send_sem=z_send.at[out, i, owner],
            recv_sem=z_recv.at[i, owner],
            device_id=at(rep, fs + step, tp), device_id_type=MESH,
        )

    def rest_copy(i, k):
        ref = piece(i, fs, lax.rem(rep + n_rep - k, n_rep))
        return pltpu.make_async_remote_copy(
            src_ref=ref, dst_ref=ref, send_sem=y_send.at[i, k - 1, fs],
            recv_sem=y_recv.at[i, k - 1, fs],
            device_id=at(rep, fs + inward, tp), device_id_type=MESH,
        )

    def y_copy(i, owner, k):
        ref = piece(i, owner, rep)
        return pltpu.make_async_remote_copy(
            src_ref=ref, dst_ref=ref, send_sem=y_send.at[i, k - 1, owner],
            recv_sem=y_recv.at[i, k - 1, owner],
            device_id=at(lax.rem(rep + k, n_rep), fs, tp), device_id_type=MESH,
        )

    def own(i):
        w = i // CUTS
        if i % CUTS == 0:
            locals_[w].wait()
        if n_fs > 1:
            z_copy(i, fs, 0).start()

        @pl.when(depth > low_depth(w))
        def _():
            z_copy(i, fs, 1).start()

    def own_end(i):
        own(i)
        for k in range(1, n_rep):
            rest_copy(i, k).start()

    def share(i, owner):
        for k in range(1, n_rep):
            y_copy(i, owner, k).start()

    def from_outer(i):
        w = i // CUTS

        def hop(h, carry):
            @pl.when((depth >= h) & (depth >= low_depth(w)))
            def _():
                owner = fs - inward * h
                z_copy(i, owner, 0).wait_recv()
                z_copy(i, owner, 0).start()
                if spread:
                    pl.when((depth > 1) | (h > 1))(lambda: share(i, owner))
                else:
                    share(i, owner)

            return carry

        lax.fori_loop(1, (n_fs + 1) // 2, hop, 0)

    def from_inner(i, start, stop):
        w = i // CUTS

        def hop(h, carry):
            @pl.when((depth + h < n_fs) & (depth >= low_depth(w)))
            def _():
                owner = fs + inward * h
                z_copy(i, owner, 1).wait_recv()

                @pl.when(depth > low_depth(w))
                def _():
                    z_copy(i, owner, 1).start()

                share(i, owner)

            return carry

        lax.fori_loop(start, stop, hop, 0)

    def near(i):
        if i < items and n_fs > 1:
            from_inner(i, 1, 2)

    def early(i):
        from_outer(i)
        if i + AHEAD < items:
            when_busy(lambda: own(i + AHEAD))
        near(i + NEAR)

    def late(i):
        if n_fs > 2:
            from_inner(i, 2, n_fs)

    def arrived_one(w, owner):
        for cut in range(CUTS):
            i = w * CUTS + cut
            for k in range(1, n_rep):
                source = lax.rem(rep + n_rep - k, n_rep)
                ref = piece(i, owner, source)
                pltpu.make_async_remote_copy(
                    src_ref=ref, dst_ref=ref, send_sem=y_send.at[i, k - 1, owner],
                    recv_sem=y_recv.at[i, k - 1, owner],
                    device_id=at(source, fs, tp), device_id_type=MESH,
                ).wait_recv()

    def arrived(w):
        def one(h, carry):
            arrived_one(w, lax.rem(fs + h, n_fs))
            return carry

        lax.fori_loop(1, n_fs, one, 0)

    def sends_done():
        def one(owner, carry):
            offset = inward * (owner - fs)
            for i in range(items):
                low = low_depth(i // CUTS)
                if n_fs > 1:
                    passed = (offset == 0) | ((offset < 0) & (depth >= low))

                    @pl.when(passed)
                    def _():
                        z_copy(i, owner, 0).wait_send()

                @pl.when((offset >= 0) & (depth > low))
                def _():
                    z_copy(i, owner, 1).wait_send()

                sent = (offset != 0) & (depth >= low)
                if spread:
                    sent = sent & ((depth != 1) | (offset != -1))

                @pl.when(sent)
                def _():
                    for k in range(1, n_rep):
                        y_copy(i, owner, k).wait_send()

            return carry

        lax.fori_loop(0, n_fs, one, 0)

        def rest():
            for i in range(items):
                for k in range(1, n_rep):
                    rest_copy(i, k).wait_send()

        when_end(rest)

    def other_chip(k):
        return lax.rem(chip + k, n_chip)

    def source_chip(k):
        return lax.rem(chip + n_chip - k, n_chip)

    def tp_copy(src, dst, send, recv, target):
        return pltpu.make_async_remote_copy(
            src_ref=src, dst_ref=dst, send_sem=send, recv_sem=recv,
            device_id=at(rep, fs, target), device_id_type=MESH,
        )

    half = block // HALVES

    def gather_copy(phase, s, k, c):
        rows = pl.ds(pl.multiple_of(core * block + c * half, half), half)
        ref = rows_all.at[s, chip, rows]
        target = other_chip(k) * 2 + core
        return tp_copy(
            ref, ref, ag_sem.at[0, phase, s, k, c], ag_sem.at[1, phase, s, k, c], target
        )

    def pass_copy(phase, s, k):
        ref = rows_all.at[s, source_chip(k), mine]
        return tp_copy(ref, ref, agf_sem.at[0, phase, s, k], agf_sem.at[1, phase, s, k], sibling)

    def gather_send(phase, s, c):
        for k in range(1, n_chip):
            gather_copy(phase, s, k, c).start()

    def gather_start(phase, s, gain):
        rows_all[s, chip, mine] = norm_rows(resid[s].astype(jnp.float32), gain[...])
        gather_send(phase, s, 0)
        pass_copy(phase, s, 0).start()

    def gather_rest(phase, s):
        for c in range(1, HALVES):
            gather_send(phase, s, c)

    def gather_pass(phase, s):
        for k in range(1, n_chip):
            for c in range(HALVES):
                gather_copy(phase, s, k, c).wait_recv()
            pass_copy(phase, s, k).start()

    def gather_in(phase, s):
        for k in range(n_chip):
            pass_copy(phase, s, k).wait_recv()

    def gather_end(phase, s):
        for k in range(1, n_chip):
            for c in range(HALVES):
                gather_copy(phase, s, k, c).wait_send()
        for k in range(n_chip):
            pass_copy(phase, s, k).wait_send()

    def each_slot(run):
        def one(s, carry):
            run(s)
            return carry

        lax.fori_loop(low_slot, 2, one, 0)

    def each_pair(run):
        def one(p, carry):
            run(p)
            return carry

        lax.fori_loop(0, n_chip, one, 0)

    def sib_copy(s, p, f):
        return tp_copy(
            to_sibling.at[s, p, f], from_sibling.at[s, p, f],
            sib_sem.at[0, s, p, f], sib_sem.at[1, s, p, f], sibling,
        )

    def chip_copy(s, k, f):
        return tp_copy(
            to_chip.at[s, k - 1, f], from_chip.at[s, k - 1, f],
            chip_sem.at[0, s, k, f], chip_sem.at[1, s, k, f], other_chip(k) * 2 + core,
        )

    def product(s, p, f, left, w):
        part[...] = jnp.dot(left[s, p], full[w][f], preferred_element_type=jnp.float32)
        to_sibling[s, p, f] = part[theirs].astype(jnp.bfloat16)
        hold[s, p, f] = part[mine]
        sib_copy(s, p, f).start()

    def products(s, f, left, w):
        def one(k, carry):
            product(s, other_chip(k), f, left, w)
            return carry

        lax.fori_loop(1, n_chip + 1, one, 0)

    def joins(s, f):
        for k in range(1, n_chip):
            p = other_chip(k)
            sib_copy(s, p, f).wait_recv()
            joined = hold[s, p, f] + from_sibling[s, p, f].astype(jnp.float32)
            to_chip[s, k - 1, f] = joined.astype(jnp.bfloat16)
            chip_copy(s, k, f).start()

    def settle(s, f):
        sib_copy(s, chip, f).wait_recv()
        total = hold[s, chip, f] + from_sibling[s, chip, f].astype(jnp.float32)
        for k in range(1, n_chip):
            chip_copy(s, k, f).wait_recv()
            total = total + from_chip[s, k - 1, f].astype(jnp.float32)
        return total

    def reduce_end(s):
        def one(f, carry):
            for k in range(1, n_chip):
                chip_copy(s, k, f).wait_send()
            for p in range(n_chip):
                sib_copy(s, p, f).wait_send()
            return carry

        lax.fori_loop(0, n_fs, one, 0)

    def band(f):
        return slice(f * cols, (f + 1) * cols)

    def project(s, p, w):
        return jnp.dot(rows_all[s, p], full[w][...], preferred_element_type=jnp.float32)

    def gate_pair(s, p):
        gate_vals[s, p] = project(s, p, GATE)

    def lift_pair(s, p):
        hidden[s, p] = (jax.nn.silu(gate_vals[s, p]) * project(s, p, LIFT)).astype(jnp.bfloat16)

    def token_copy():
        return pltpu.make_async_remote_copy(
            src_ref=stream, dst_ref=resid.at[0], send_sem=token_sem.at[0],
            recv_sem=token_sem.at[1], device_id=at(rep, fs + inward, tp), device_id_type=MESH,
        )

    def second_copy(f):
        return pltpu.make_async_remote_copy(
            src_ref=resid.at[0, :, band(f)], dst_ref=resid.at[1, :, band(f)],
            send_sem=second_sem.at[0, f], recv_sem=second_sem.at[1, f],
            device_id=at(rep, fs - inward, tp), device_id_type=MESH,
        )

    def feed():
        token_copy().start()
        for i in range(items):
            own_end(i)

    when_end(feed)

    def open_own():
        for i in range(AHEAD):
            own(i)
        resid[1] = stream[...]
        gather_start(0, 1, gain_before)
        gather_rest(0, 1)

    when_busy(open_own)
    for i in range(NEAR):
        near(i)

    def open_guest():
        token_copy().wait_recv()
        gather_start(0, 0, gain_before)
        gather_rest(0, 0)

    def nth_owner(j):
        near = jnp.maximum(depth - j, 0) + j * jnp.minimum(jnp.maximum(j - depth, 0), 1)
        return near + side * (n_fs - 1 - 2 * near)

    def serve_all(w):
        for i in range(w * CUTS, (w + 1) * CUTS):
            serve(i)

    when_mid(open_guest)

    def gates():
        each_slot(lambda s: gather_in(0, s))
        arrived(GATE)
        each_slot(lambda s: each_pair(lambda p: gate_pair(s, p)))

    def lifts(s):
        each_pair(lambda p: lift_pair(s, p))
        gather_end(0, s)

    def lifts_own():
        arrived(LIFT)
        lifts(1)

    def down_block(owner):
        each_slot(lambda s: products(s, owner, hidden, DOWN))
        each_slot(lambda s: joins(s, owner))

    def downs(start, stop):
        def one(j, carry):
            owner = nth_owner(j)
            arrived_one(DOWN, owner)
            down_block(owner)
            return carry

        lax.fori_loop(start, stop, one, 0)

    def firsts():
        def one(s):
            for f in range(n_fs):
                base = resid[s, :, band(f)].astype(jnp.float32)
                resid[s, :, band(f)] = (base + 0.5 * settle(s, f)).astype(jnp.bfloat16)
            reduce_end(s)
            gather_start(1, s, mixer_gain)
            if spread:
                pl.when((s == 0) | (depth != 1))(lambda: gather_rest(1, s))
            else:
                gather_rest(1, s)

        each_slot(one)

    def guest_lifts():
        when_mid(lambda: lifts(0))
        when_busy(lambda: down_block(fs))

    stops = [1 + (n_fs - 1) * t // 3 for t in range(4)]
    first_down = MIX_U * CUTS
    between = {
        GATE * CUTS: lambda: when_busy(lambda: gather_pass(0, 1)),
        GATE * CUTS + 1: lambda: when_mid(lambda: gather_pass(0, 0)),
        LIFT * CUTS + 1: lambda: when_busy(gates),
        DOWN * CUTS: lambda: when_busy(lifts_own),
        DOWN * CUTS + 1: guest_lifts,
        first_down: lambda: when_busy(lambda: downs(stops[0], stops[1])),
        first_down + 1: lambda: when_busy(lambda: downs(stops[1], stops[2])),
        first_down + 2: lambda: when_busy(lambda: downs(stops[2], stops[3])),
        first_down + 3: lambda: when_busy(firsts),
    }
    for i in range(items):
        early(i)
        if i in between:
            between[i]()
        late(i)

    groups = spatial.shape[0]
    channels = lifted.shape[3]
    group_dim = channels // groups
    all_channels = channels * n_tp

    def u_pair(s, p):
        u_vals[s, p] = jax.nn.gelu(project(s, p, MIX_U))

    def v_pair(s, p):
        values = jax.nn.gelu(project(s, p, MIX_V))
        lifted[s, p] = values
        sums = jnp.sum(values, axis=1, keepdims=True)
        squares = jnp.sum(values * values, axis=1, keepdims=True)
        lane = lax.broadcasted_iota(jnp.int32, (pair, 128), 1)
        both = jnp.where(lane == 0, sums, jnp.where(lane == 1, squares, 0.0))
        mom_own[s, p] = both.T[:8]

    def mom_copy(s, k):
        return tp_copy(
            mom_own.at[s], mom_in.at[s, k - 1], mom_sem.at[0, s, k], mom_sem.at[1, s, k],
            lax.rem(tp + k, n_tp),
        )

    def values_of(s):
        gather_pass(1, s)
        gather_in(1, s)
        each_pair(lambda p: u_pair(s, p))
        each_pair(lambda p: v_pair(s, p))
        for k in range(1, n_tp):
            mom_copy(s, k).start()
        gather_end(1, s)

    def mix_of(s):
        for k in range(1, n_tp):
            mom_copy(s, k).wait_recv()
        shift_columns = square[...].T

        def mix_pair(p):
            moments = mom_own[s, p]
            for k in range(1, n_tp):
                moments = moments + mom_in[s, k - 1, p]
            moments = moments * (1.0 / all_channels)
            columns = jnp.concatenate([moments, jnp.zeros((120, pair), jnp.float32)], axis=0).T
            centre = columns[:, 0:1]
            spread_of = columns[:, 1:2] - centre * centre
            normed_v = (
                (lifted[s, p] - centre) * lax.rsqrt(spread_of + layer_epsilon) * layer_gain[...]
                + layer_shift[...]
            ).astype(jnp.bfloat16)
            for g in range(groups):
                cut = slice(g * group_dim, (g + 1) * group_dim)
                for b in range(pair // SPAN):
                    span = slice(b * SPAN, (b + 1) * SPAN)
                    mixed = jnp.dot(
                        masked[g], normed_v[span, cut], preferred_element_type=jnp.float32
                    )
                    mixed = mixed + shift_columns[:, g : g + 1]
                    gated[s, p, span, cut] = (u_vals[s, p, span, cut] * mixed).astype(jnp.bfloat16)

        each_pair(mix_pair)
        for k in range(1, n_tp):
            mom_copy(s, k).wait_send()

    def mixer_in():
        row = lax.broadcasted_iota(jnp.int32, (SPAN, SPAN), 0)
        col = lax.broadcasted_iota(jnp.int32, (SPAN, SPAN), 1)
        for g in range(groups):
            masked[g] = jnp.where(row >= col, spatial[g].astype(jnp.float32), 0.0).astype(
                jnp.bfloat16
            )
        square[...] = jnp.zeros_like(square)
        square[0:groups, :] = spatial_shift[...]
        arrived(MIX_U)
        arrived(MIX_V)

    when_busy(mixer_in)

    def span_of(s, start, stop):
        def over(run):
            def one(h, carry):
                run(lax.rem(fs + h, n_fs))
                return carry

            lax.fori_loop(start, stop, one, 0)

        over(lambda f: products(s, f, gated, MIX_DOWN))
        over(lambda f: joins(s, f))

    def mixer_out():
        middle = n_fs // 2

        def guest_in():
            values_of(0)
            gather_rest(1, 1)
            mix_of(0)
            arrived(MIX_DOWN)
            span_of(0, 0, middle)

        def guest_rest():
            span_of(0, middle, n_fs)

        when_mid(guest_in)
        values_of(1)
        if spread:
            pl.when(depth > 1)(lambda: arrived(MIX_DOWN))
        else:
            arrived(MIX_DOWN)
        when_mid(guest_rest)
        mix_of(1)
        span_of(1, 0, n_fs)

        def second(s, f):
            base = resid[s, :, band(f)].astype(jnp.float32)
            resid[s, :, band(f)] = (base + settle(s, f)).astype(jnp.bfloat16)

        def guest():
            for f in range(n_fs):
                second(0, f)
                second_copy(f).start()
            reduce_end(0)

        when_mid(guest)
        for f in range(n_fs):
            second(1, f)
        reduce_end(1)

    when_busy(mixer_out)

    def close_guest():
        arrived(GATE)
        arrived(LIFT)
        arrived(DOWN)
        for f in range(n_fs):
            second_copy(f).wait_recv()

    when_end(close_guest)
    def gather_half(k, c):
        ref = rows_last.at[chip, c, core]
        target = other_chip(k) * 2 + core
        return tp_copy(ref, ref, agl_sem.at[0, k, c], agl_sem.at[1, k, c], target)

    def pass_half(k, c):
        ref = rows_last.at[source_chip(k), c, core]
        return tp_copy(ref, ref, agl_sem.at[2, k, c], agl_sem.at[3, k, c], sibling)

    def sib_half(p, f, c):
        rows = pl.ds(c * half, half)
        return tp_copy(
            to_sibling.at[1, p, f, rows], from_sibling.at[1, p, f, rows],
            last_sem.at[0, p, f, c], last_sem.at[1, p, f, c], sibling,
        )

    def chip_half(k, f, c):
        rows = pl.ds(c * half, half)
        return tp_copy(
            to_chip.at[1, k - 1, f, rows], from_chip.at[1, k - 1, f, rows],
            last_sem.at[2, k, f, c], last_sem.at[3, k, f, c], other_chip(k) * 2 + core,
        )

    normed = norm_rows(resid[1].astype(jnp.float32), gain_after[...])
    for c in range(HALVES):
        rows_last[chip, c, core] = normed[c * half : (c + 1) * half]
        for k in range(1, n_chip):
            gather_half(k, c).start()
        pass_half(0, c).start()

    def last_rows(p, c):
        rows = rows_last[p, c].reshape(2 * half, width)
        gate = jnp.dot(rows, full[GATE][...], preferred_element_type=jnp.float32)
        lift = jnp.dot(rows, full[LIFT][...], preferred_element_type=jnp.float32)
        hidden_last[p, c] = (jax.nn.silu(gate) * lift).astype(jnp.bfloat16)

    def last_products(p, c):
        def one(f, carry):
            part_half[...] = jnp.dot(
                hidden_last[p, c], full[DOWN][f], preferred_element_type=jnp.float32
            ).reshape(part_half.shape)
            rows = pl.ds(c * half, half)
            to_sibling[1, p, f, rows] = part_half[1 - core].astype(jnp.bfloat16)
            hold[1, p, f, rows] = part_half[core]
            sib_half(p, f, c).start()
            return carry

        lax.fori_loop(0, n_fs, one, 0)

    def last_joins(k, c):
        p = other_chip(k)

        def one(f, carry):
            rows = pl.ds(c * half, half)
            sib_half(p, f, c).wait_recv()
            joined = hold[1, p, f, rows] + from_sibling[1, p, f, rows].astype(jnp.float32)
            to_chip[1, k - 1, f, rows] = joined.astype(jnp.bfloat16)
            chip_half(k, f, c).start()
            return carry

        lax.fori_loop(0, n_fs, one, 0)

    for c in range(HALVES):
        pass_half(0, c).wait_recv()
        last_rows(chip, c)
    for c in range(HALVES):
        for k in range(1, n_chip):
            gather_half(k, c).wait_recv()
            pass_half(k, c).start()
        for k in range(1, n_chip):
            pass_half(k, c).wait_recv()
            last_rows(other_chip(k), c)
            if c > 0:
                last_joins(k, c - 1)
            last_products(other_chip(k), c)
    last_products(chip, 0)
    for k in range(1, n_chip):
        last_joins(k, HALVES - 1)
    for c in range(1, HALVES):
        last_products(chip, c)
    for f in range(n_fs):
        for c in range(HALVES):
            sib_half(chip, f, c).wait_recv()
        total = hold[1, chip, f] + from_sibling[1, chip, f].astype(jnp.float32)
        for k in range(1, n_chip):
            for c in range(HALVES):
                chip_half(k, f, c).wait_recv()
            total = total + from_chip[1, k - 1, f].astype(jnp.float32)
        base = resid[1, :, band(f)].astype(jnp.float32)
        out[:, band(f)] = (base + 0.5 * total).astype(jnp.bfloat16)
    for c in range(HALVES):
        for k in range(n_chip):
            pass_half(k, c).wait_send()
        for k in range(1, n_chip):
            gather_half(k, c).wait_send()

    def last_sent(f, carry):
        for c in range(HALVES):
            for p in range(n_chip):
                sib_half(p, f, c).wait_send()
            for k in range(1, n_chip):
                chip_half(k, f, c).wait_send()
        return carry

    lax.fori_loop(0, n_fs, last_sent, 0)
    when_end(lambda: token_copy().wait_send())

    def shipped():
        for f in range(n_fs):
            second_copy(f).wait_send()

    when_mid(shipped)
    sends_done()


def body(
    n_rep,
    n_fs,
    n_tp,
    stream,
    gain_before,
    gain_after,
    proj_gate,
    proj_lift,
    proj_down,
    mixer_gain,
    mixer_u,
    mixer_v,
    layer_gain,
    layer_shift,
    spatial,
    spatial_shift,
    mixer_down,
):
    block, width = stream.shape
    n_chip = n_tp // 2
    pair = 2 * block
    cols = width // n_fs
    units = proj_gate.shape[1]
    channels = mixer_u.shape[1]
    bf16, f32 = jnp.bfloat16, jnp.float32
    shards = (proj_gate, proj_lift, proj_down, mixer_u, mixer_v, mixer_down)
    vmem = pl.BlockSpec(memory_space=pltpu.VMEM)
    anywhere = pl.BlockSpec(memory_space=pl.ANY)
    dma = pltpu.SemaphoreType.DMA
    spread_reps = max(n_rep - 1, 1)
    spread_chips = max(n_chip - 1, 1)
    return pl.pallas_call(
        functools.partial(layer_kernel, n_rep, n_fs, n_tp),
        out_shape=jax.ShapeDtypeStruct((block, width), bf16),
        in_specs=[vmem] * 8 + [anywhere] * 6,
        out_specs=vmem,
        scratch_shapes=[
            pltpu.VMEM(
                (n_fs * w.shape[0], w.shape[1]) if i in BY_ROWS else (n_fs,) + w.shape, bf16
            )
            for i, w in enumerate(shards)
        ]
        + [
            pltpu.VMEM((2, n_chip, pair, width), bf16),
            pltpu.VMEM((2, n_chip, n_fs, block, cols), bf16),
            pltpu.VMEM((2, n_chip, n_fs, block, cols), bf16),
            pltpu.VMEM((2, spread_chips, n_fs, block, cols), bf16),
            pltpu.VMEM((2, spread_chips, n_fs, block, cols), bf16),
            pltpu.VMEM((pair, cols), f32),
            pltpu.VMEM((2, n_chip, n_fs, block, cols), f32),
            pltpu.VMEM((2, n_chip, pair, units), f32),
            pltpu.VMEM((2, n_chip, pair, units), bf16),
            pltpu.VMEM((2, n_chip, pair, channels), f32),
            pltpu.VMEM((2, n_chip, pair, channels), f32),
            pltpu.VMEM((2, n_chip, pair, channels), bf16),
            pltpu.VMEM((n_chip, HALVES, 2, block // HALVES, width), bf16),
            pltpu.VMEM((n_chip, HALVES, 2 * block // HALVES, units), bf16),
            pltpu.VMEM((2, block // HALVES, cols), f32),
            pltpu.VMEM(spatial.shape, bf16),
            pltpu.VMEM((2, n_chip, 8, pair), f32),
            pltpu.VMEM((2, max(n_tp - 1, 1), n_chip, 8, pair), f32),
            pltpu.VMEM((128, SPAN), f32),
            pltpu.VMEM((2, block, width), bf16),
            dma((6,)),
            dma((2, 6 * CUTS, n_fs)),
            dma((6 * CUTS, n_fs)),
            dma((6 * CUTS, spread_reps, n_fs)),
            dma((6 * CUTS, spread_reps, n_fs)),
            dma((2, 2, 2, n_chip, HALVES)),
            dma((2, 2, 2, n_chip)),
            dma((2, 2, n_chip, n_fs)),
            dma((2, 2, n_chip, n_fs)),
            dma((2, 2, n_tp)),
            dma((2,)),
            dma((2, n_fs)),
            dma((4, n_chip, HALVES)),
            dma((4, n_chip, n_fs, HALVES)),
        ],
        compiler_params=pltpu.CompilerParams(
            collective_id=0, has_side_effects=True, vmem_limit_bytes=60 * 1024 * 1024
        ),
    )(
        stream,
        gain_before.reshape(1, -1),
        gain_after.reshape(1, -1),
        mixer_gain.reshape(1, -1),
        layer_gain.reshape(1, -1),
        layer_shift.reshape(1, -1),
        spatial,
        spatial_shift,
        *shards,
    )


def solution(mesh):
    placed = (
        P(("rep", "fs", "tp"), None),
        P(),
        P(),
        P("fs", "tp"),
        P("fs", "tp"),
        P("tp", "fs"),
        P(),
        P("fs", "tp"),
        P("fs", "tp"),
        P("tp"),
        P("tp"),
        P("tp", None, None),
        P("tp", None),
        P("tp", "fs"),
    )
    sizes = (mesh.shape["rep"], mesh.shape["fs"], mesh.shape["tp"])
    return jax.shard_map(
        functools.partial(body, *sizes),
        mesh=mesh,
        in_specs=placed,
        out_specs=P(("rep", "fs", "tp"), None),
        check_vma=False,
    )
```

time: 229 us -> 188 us (0.82)
  the two profiles are of different devices: /device:TPU:0 before, /device:TPU:16 now
where the time goes in v1:
time: 188 us; the launch traced here: 186 us
  Pallas kernels  184 us (98%)
    pallas_call x1, Pallas kernels, body(): pl.pallas_call(functools.partial(layer_kernel, n_rep, n_fs, n_tp), out_sh...  184 us

profile of v1, /device:TPU:16, one launch (start us, length us, event | category | flops | bytes accessed | tf_op | source)
XLA Modules:
  0.0 186.3 jit_solution(9236744949868107507)
XLA Ops:
  0.0 184.4 %shard_map.136 = bf16[128,2048]{1,0:T(8,128)(2,1)} custom-call(bf16[128,2048]{1,0:T(8,128)(2,1)} %stream.1, f32[1,2048]{1,0:T(1,128)} %bitcast.5, f32[1,2048]{1,0:T(1,128)} %bitcast.6, f32[1,2048]{1,0:T(1,128)} %bitcast.7, f32[1,512]{1,0:T(1,128)} %bitcast.8, f32[1,512]{1,0:T(1,128)} %bitcast.9, bf16[4,128,128]{2,1,0:T(8,128)(2,1)} %spatial.1, ...), custom_call_target="tpu_custom_call" | custom-call | tf_op jit(solution)/shard_map/pallas_call | solution.py:857
  184.4 1.9 %copy.16 = bf16[128,2048]{1,0:T(8,128)(2,1)} copy(bf16[128,2048]{1,0:T(8,128)(2,1)} %shard_map.136) | data formatting | bytes 1048576

commit v2 on v1

--- a/solution.py
+++ b/solution.py
@@ -14,12 +14,13 @@
 
 MESH = pl.DeviceIdType.MESH
 GATE, LIFT, DOWN, MIX_U, MIX_V, MIX_DOWN = range(6)
-CUTS = 2
-AHEAD = 3
-NEAR = 1
 HALVES = 2
 MIXERS = (MIX_U, MIX_V, MIX_DOWN)
 BY_ROWS = (GATE, LIFT, MIX_U, MIX_V)
+
+
+def cuts_of(shards, n_rep):
+    return 2 if all(w.shape[0] % (n_rep * 32) == 0 for w in shards) else 1
 
 
 def norm_rows(widened, scale_gain):
@@ -94,6 +95,8 @@
     pair = 2 * block
     cols = width // n_fs
     shards = (proj_gate, proj_lift, proj_down, mixer_u, mixer_v, mixer_down)
+    cuts = cuts_of(shards, n_rep)
+    ahead, near_by = cuts + 2, cuts
     full = (gate_all, lift_all, down_all, u_all, v_all, mix_down_all)
     mine = pl.ds(pl.multiple_of(core * block, block), block)
     theirs = pl.ds(pl.multiple_of((1 - core) * block, block), block)
@@ -167,12 +170,12 @@
     line_peers = jnp.minimum(fs, 1) + jnp.minimum(n_fs - 1 - fs, 1)
     pl.semaphore_wait(barrier, n_rep - 1 + n_tp - 1 + line_peers)
 
-    items = 6 * CUTS
+    items = 6 * cuts
 
     def piece(i, owner, part_index):
-        w, cut = i // CUTS, i % CUTS
-        rows = depth_of(w) // (n_rep * CUTS)
-        first_row = (part_index * CUTS + cut) * rows
+        w, cut = i // cuts, i % cuts
+        rows = depth_of(w) // (n_rep * cuts)
+        first_row = (part_index * cuts + cut) * rows
         if w in BY_ROWS:
             start = pl.multiple_of(owner * depth_of(w) + first_row, rows)
             return full[w].at[pl.ds(start, rows)]
@@ -204,8 +207,8 @@
         )
 
     def own(i):
-        w = i // CUTS
-        if i % CUTS == 0:
+        w = i // cuts
+        if i % cuts == 0:
             locals_[w].wait()
         if n_fs > 1:
             z_copy(i, fs, 0).start()
@@ -214,8 +217,7 @@
         def _():
             z_copy(i, fs, 1).start()
 
-    def own_end(i):
-        own(i)
+    def rest_end(i):
         for k in range(1, n_rep):
             rest_copy(i, k).start()
 
@@ -224,7 +226,7 @@
             y_copy(i, owner, k).start()
 
     def from_outer(i):
-        w = i // CUTS
+        w = i // cuts
 
         def hop(h, carry):
             @pl.when((depth >= h) & (depth >= low_depth(w)))
@@ -242,7 +244,7 @@
         lax.fori_loop(1, (n_fs + 1) // 2, hop, 0)
 
     def from_inner(i, start, stop):
-        w = i // CUTS
+        w = i // cuts
 
         def hop(h, carry):
             @pl.when((depth + h < n_fs) & (depth >= low_depth(w)))
@@ -266,17 +268,20 @@
 
     def early(i):
         from_outer(i)
-        if i + AHEAD < items:
-            when_busy(lambda: own(i + AHEAD))
-        near(i + NEAR)
+        if i < MIX_U * cuts - near_by:
+            near(i + near_by)
+        elif i >= MIX_U * cuts - 1:
+            near(i + 1)
 
     def late(i):
         if n_fs > 2:
             from_inner(i, 2, n_fs)
+        if i + ahead < items:
+            when_busy(lambda: own(i + ahead))
 
     def arrived_one(w, owner):
-        for cut in range(CUTS):
-            i = w * CUTS + cut
+        for cut in range(cuts):
+            i = w * cuts + cut
             for k in range(1, n_rep):
                 source = lax.rem(rep + n_rep - k, n_rep)
                 ref = piece(i, owner, source)
@@ -297,7 +302,7 @@
         def one(owner, carry):
             offset = inward * (owner - fs)
             for i in range(items):
-                low = low_depth(i // CUTS)
+                low = low_depth(i // cuts)
                 if n_fs > 1:
                     passed = (offset == 0) | ((offset < 0) & (depth >= low))
 
@@ -451,7 +456,7 @@
         lax.fori_loop(0, n_fs, one, 0)
 
     def band(f):
-        return slice(f * cols, (f + 1) * cols)
+        return pl.ds(pl.multiple_of(f * cols, cols), cols)
 
     def project(s, p, w):
         return jnp.dot(rows_all[s, p], full[w][...], preferred_element_type=jnp.float32)
@@ -477,20 +482,23 @@
 
     def feed():
         token_copy().start()
-        for i in range(items):
-            own_end(i)
+        for w in range(6):
+            for i in range(w * cuts, (w + 1) * cuts):
+                own(i)
+            for i in range(w * cuts, (w + 1) * cuts):
+                rest_end(i)
 
     when_end(feed)
 
     def open_own():
-        for i in range(AHEAD):
+        for i in range(ahead):
             own(i)
         resid[1] = stream[...]
         gather_start(0, 1, gain_before)
         gather_rest(0, 1)
 
     when_busy(open_own)
-    for i in range(NEAR):
+    for i in range(near_by):
         near(i)
 
     def open_guest():
@@ -499,12 +507,12 @@
         gather_rest(0, 0)
 
     def nth_owner(j):
-        near = jnp.maximum(depth - j, 0) + j * jnp.minimum(jnp.maximum(j - depth, 0), 1)
-        return near + side * (n_fs - 1 - 2 * near)
-
-    def serve_all(w):
-        for i in range(w * CUTS, (w + 1) * CUTS):
-            serve(i)
+        beyond = jnp.maximum(j - 1, 0)
+        outs = jnp.minimum(beyond, depth)
+        ins = beyond - outs
+        first, far = jnp.minimum(beyond, 1), jnp.minimum(ins, 1)
+        offset = (1 - first) * jnp.minimum(j, 1) + far * (ins + 1) - (first - far) * outs
+        return fs + inward * offset
 
     when_mid(open_guest)
 
@@ -520,6 +528,8 @@
     def lifts_own():
         arrived(LIFT)
         lifts(1)
+        products(1, fs, hidden, DOWN)
+        joins(1, fs)
 
     def down_block(owner):
         each_slot(lambda s: products(s, owner, hidden, DOWN))
@@ -534,42 +544,48 @@
 
         lax.fori_loop(start, stop, one, 0)
 
-    def firsts():
-        def one(s):
-            for f in range(n_fs):
-                base = resid[s, :, band(f)].astype(jnp.float32)
-                resid[s, :, band(f)] = (base + 0.5 * settle(s, f)).astype(jnp.bfloat16)
-            reduce_end(s)
-            gather_start(1, s, mixer_gain)
-            if spread:
-                pl.when((s == 0) | (depth != 1))(lambda: gather_rest(1, s))
-            else:
-                gather_rest(1, s)
-
-        each_slot(one)
+    def first_band(s, j):
+        f = nth_owner(j)
+        base = resid[s, :, band(f)].astype(jnp.float32)
+        resid[s, :, band(f)] = (base + 0.5 * settle(s, f)).astype(jnp.bfloat16)
+
+    def first_bands(s, start, stop):
+        def one(j, carry):
+            first_band(s, j)
+            return carry
+
+        lax.fori_loop(start, stop, one, 0)
+
+    def last_downs():
+        downs(stops[2], stops[3])
+        each_slot(lambda s: first_bands(s, 0, n_fs - 1))
+
+    def first_of(s):
+        first_bands(s, n_fs - 1, n_fs)
+        gather_start(1, s, mixer_gain)
+
+    def guest_first():
+        first_of(0)
+        gather_rest(1, 0)
+
+    def own_first():
+        first_of(1)
+        if spread:
+            pl.when(depth != 1)(lambda: gather_rest(1, 1))
+        else:
+            gather_rest(1, 1)
+        each_slot(reduce_end)
 
     def guest_lifts():
-        when_mid(lambda: lifts(0))
-        when_busy(lambda: down_block(fs))
+        lifts(0)
+        products(0, fs, hidden, DOWN)
+        joins(0, fs)
 
     stops = [1 + (n_fs - 1) * t // 3 for t in range(4)]
-    first_down = MIX_U * CUTS
-    between = {
-        GATE * CUTS: lambda: when_busy(lambda: gather_pass(0, 1)),
-        GATE * CUTS + 1: lambda: when_mid(lambda: gather_pass(0, 0)),
-        LIFT * CUTS + 1: lambda: when_busy(gates),
-        DOWN * CUTS: lambda: when_busy(lifts_own),
-        DOWN * CUTS + 1: guest_lifts,
-        first_down: lambda: when_busy(lambda: downs(stops[0], stops[1])),
-        first_down + 1: lambda: when_busy(lambda: downs(stops[1], stops[2])),
-        first_down + 2: lambda: when_busy(lambda: downs(stops[2], stops[3])),
-        first_down + 3: lambda: when_busy(firsts),
-    }
-    for i in range(items):
-        early(i)
-        if i in between:
-            between[i]()
-        late(i)
+
+    def far_downs():
+        downs(stops[2], stops[3])
+        each_slot(lambda s: first_bands(s, 0, n_fs - 1))
 
     groups = spatial.shape[0]
     channels = lifted.shape[3]
@@ -634,6 +650,10 @@
         for k in range(1, n_tp):
             mom_copy(s, k).wait_send()
 
+    def guest_values():
+        values_of(0)
+        gather_rest(1, 1)
+
     def mixer_in():
         row = lax.broadcasted_iota(jnp.int32, (SPAN, SPAN), 0)
         col = lax.broadcasted_iota(jnp.int32, (SPAN, SPAN), 1)
@@ -645,32 +665,67 @@
         square[0:groups, :] = spatial_shift[...]
         arrived(MIX_U)
         arrived(MIX_V)
-
-    when_busy(mixer_in)
+        when_mid(guest_values)
+
+
+    between = {
+        (GATE, 0): lambda: when_busy(lambda: gather_pass(0, 1)),
+        (GATE, 3): lambda: when_mid(lambda: gather_pass(0, 0)),
+        (LIFT, 2): lambda: when_busy(gates),
+        (DOWN, 0): lambda: when_busy(lifts_own),
+        (DOWN, 1): lambda: when_mid(guest_lifts),
+        (DOWN, 2): lambda: when_busy(lambda: downs(stops[0], stops[1])),
+        (DOWN, 3): lambda: when_busy(lambda: downs(stops[1], stops[2])),
+        (MIX_U, 1): lambda: when_busy(far_downs),
+        (MIX_U, 3): lambda: when_mid(guest_first),
+        (MIX_V, 1): lambda: when_busy(own_first),
+        (MIX_DOWN, 1): lambda: when_busy(mixer_in),
+    }
+    for w in range(6):
+        for stage, step in enumerate((early, late)):
+            for i in range(w * cuts, (w + 1) * cuts):
+                step(i)
+                for place, edge in enumerate((w * cuts, (w + 1) * cuts - 1)):
+                    if i == edge and (w, 2 * stage + place) in between:
+                        between[w, 2 * stage + place]()
+
+    def bands_of(start, stop, run):
+        def one(h, carry):
+            run(lax.rem(fs + h, n_fs))
+            return carry
+
+        lax.fori_loop(start, stop, one, 0)
 
     def span_of(s, start, stop):
-        def over(run):
-            def one(h, carry):
-                run(lax.rem(fs + h, n_fs))
-                return carry
-
-            lax.fori_loop(start, stop, one, 0)
-
-        over(lambda f: products(s, f, gated, MIX_DOWN))
-        over(lambda f: joins(s, f))
+        bands_of(start, stop, lambda f: products(s, f, gated, MIX_DOWN))
+        bands_of(start, stop, lambda f: joins(s, f))
+
+    def second_band(s, f):
+        base = resid[s, :, band(f)].astype(jnp.float32)
+        resid[s, :, band(f)] = (base + settle(s, f)).astype(jnp.bfloat16)
+
+    def ship(start, stop):
+        def one(f):
+            second_band(0, f)
+            second_copy(f).start()
+
+        bands_of(start, stop, one)
 
     def mixer_out():
         middle = n_fs // 2
 
         def guest_in():
-            values_of(0)
-            gather_rest(1, 1)
             mix_of(0)
             arrived(MIX_DOWN)
             span_of(0, 0, middle)
 
         def guest_rest():
             span_of(0, middle, n_fs)
+            ship(0, middle)
+
+        def guest_ship():
+            ship(middle, n_fs)
+            reduce_end(0)
 
         when_mid(guest_in)
         values_of(1)
@@ -681,20 +736,8 @@
         when_mid(guest_rest)
         mix_of(1)
         span_of(1, 0, n_fs)
-
-        def second(s, f):
-            base = resid[s, :, band(f)].astype(jnp.float32)
-            resid[s, :, band(f)] = (base + settle(s, f)).astype(jnp.bfloat16)
-
-        def guest():
-            for f in range(n_fs):
-                second(0, f)
-                second_copy(f).start()
-            reduce_end(0)
-
-        when_mid(guest)
-        for f in range(n_fs):
-            second(1, f)
+        when_mid(guest_ship)
+        bands_of(0, n_fs, lambda f: second_band(1, f))
         reduce_end(1)
 
     when_busy(mixer_out)
@@ -779,14 +822,10 @@
         for k in range(1, n_chip):
             pass_half(k, c).wait_recv()
             last_rows(other_chip(k), c)
-            if c > 0:
-                last_joins(k, c - 1)
             last_products(other_chip(k), c)
-    last_products(chip, 0)
-    for k in range(1, n_chip):
-        last_joins(k, HALVES - 1)
-    for c in range(1, HALVES):
         last_products(chip, c)
+        for k in range(1, n_chip):
+            last_joins(k, c)
     for f in range(n_fs):
         for c in range(HALVES):
             sib_half(chip, f, c).wait_recv()
@@ -849,6 +888,7 @@
     channels = mixer_u.shape[1]
     bf16, f32 = jnp.bfloat16, jnp.float32
     shards = (proj_gate, proj_lift, proj_down, mixer_u, mixer_v, mixer_down)
+    cuts = cuts_of(shards, n_rep)
     vmem = pl.BlockSpec(memory_space=pltpu.VMEM)
     anywhere = pl.BlockSpec(memory_space=pl.ANY)
     dma = pltpu.SemaphoreType.DMA
@@ -856,7 +896,7 @@
     spread_chips = max(n_chip - 1, 1)
     return pl.pallas_call(
         functools.partial(layer_kernel, n_rep, n_fs, n_tp),
-        out_shape=jax.ShapeDtypeStruct((block, width), bf16),
+        out_shape=pltpu.VMEM((block, width), bf16),
         in_specs=[vmem] * 8 + [anywhere] * 6,
         out_specs=vmem,
         scratch_shapes=[
@@ -887,10 +927,10 @@
             pltpu.VMEM((128, SPAN), f32),
             pltpu.VMEM((2, block, width), bf16),
             dma((6,)),
-            dma((2, 6 * CUTS, n_fs)),
-            dma((6 * CUTS, n_fs)),
-            dma((6 * CUTS, spread_reps, n_fs)),
-            dma((6 * CUTS, spread_reps, n_fs)),
+            dma((2, 6 * cuts, n_fs)),
+            dma((6 * cuts, n_fs)),
+            dma((6 * cuts, spread_reps, n_fs)),
+            dma((6 * cuts, spread_reps, n_fs)),
             dma((2, 2, 2, n_chip, HALVES)),
             dma((2, 2, 2, n_chip)),
             dma((2, 2, n_chip, n_fs)),

time: 188 us -> 178 us (0.947)
  Pallas kernels: 184 us -> 176 us
    pallas_call x1, Pallas kernels: 184 us -> 176 us  [body(): pl.pallas_call(functools.partial(layer_kernel, n_rep, n_fs, n_tp), out_sh...]
where the time goes in v2:
time: 178 us; the launch traced here: 177 us
  Pallas kernels  176 us (99%)
    pallas_call x1, Pallas kernels, body(): pl.pallas_call(functools.partial(layer_kernel, n_rep, n_fs, n_tp), out_sh...  176 us

profile of v2, /device:TPU:16, one launch (start us, length us, event | category | flops | bytes accessed | tf_op | source)
XLA Modules:
  0.0 177.2 jit_solution(2795197575635840620)
XLA Ops:
  0.0 176.4 %shard_map.136 = bf16[128,2048]{1,0:T(8,128)(2,1)S(1)} custom-call(bf16[128,2048]{1,0:T(8,128)(2,1)} %stream.1, f32[1,2048]{1,0:T(1,128)} %bitcast.5, f32[1,2048]{1,0:T(1,128)} %bitcast.6, f32[1,2048]{1,0:T(1,128)} %bitcast.7, f32[1,512]{1,0:T(1,128)} %bitcast.8, f32[1,512]{1,0:T(1,128)} %bitcast.9, bf16[4,128,128]{2,1,0:T(8,128)(2,1)} %spatial.1, ...), custom_call_target="tpu_custom_call" | custom-call | tf_op jit(solution)/shard_map/pallas_call | solution.py:897
  176.4 0.8 copy.16

commit v3 on v2

--- a/solution.py
+++ b/solution.py
@@ -75,6 +75,7 @@
     resid,
     local_sem,
     z_send,
+    out_send,
     z_recv,
     y_send,
     y_recv,
@@ -85,8 +86,6 @@
     mom_sem,
     token_sem,
     second_sem,
-    agl_sem,
-    last_sem,
 ):
     rep, fs, tp = lax.axis_index("rep"), lax.axis_index("fs"), lax.axis_index("tp")
     chip, core = tp // 2, lax.rem(tp, 2)
@@ -172,20 +171,33 @@
 
     items = 6 * cuts
 
-    def piece(i, owner, part_index):
-        w, cut = i // cuts, i % cuts
-        rows = depth_of(w) // (n_rep * cuts)
-        first_row = (part_index * cuts + cut) * rows
+    def rows_of(w, owner, first_row, rows):
         if w in BY_ROWS:
             start = pl.multiple_of(owner * depth_of(w) + first_row, rows)
             return full[w].at[pl.ds(start, rows)]
         return full[w].at[owner, pl.ds(pl.multiple_of(first_row, rows), rows)]
 
-    def z_copy(i, owner, out):
+    def piece(i, owner, part_index):
+        w, cut = i // cuts, i % cuts
+        rows = depth_of(w) // (n_rep * cuts)
+        return rows_of(w, owner, (part_index * cuts + cut) * rows, rows)
+
+    def share_of(w, owner, part_index):
+        rows = depth_of(w) // n_rep
+        return rows_of(w, owner, part_index * rows, rows)
+
+    def settled(ref, send, recv):
+        return pltpu.make_async_remote_copy(
+            src_ref=ref, dst_ref=ref, send_sem=send, recv_sem=recv,
+            device_id=at(lax.rem(rep + 1, n_rep), fs, tp), device_id_type=MESH,
+        )
+
+    def z_copy(i, owner, out, own_out=False):
         ref = piece(i, owner, rep)
         step = inward if out == 0 else -inward
+        sem = out_send.at[i // cuts] if own_out else z_send.at[i // cuts, owner]
         return pltpu.make_async_remote_copy(
-            src_ref=ref, dst_ref=ref, send_sem=z_send.at[out, i, owner],
+            src_ref=ref, dst_ref=ref, send_sem=sem,
             recv_sem=z_recv.at[i, owner],
             device_id=at(rep, fs + step, tp), device_id_type=MESH,
         )
@@ -193,16 +205,16 @@
     def rest_copy(i, k):
         ref = piece(i, fs, lax.rem(rep + n_rep - k, n_rep))
         return pltpu.make_async_remote_copy(
-            src_ref=ref, dst_ref=ref, send_sem=y_send.at[i, k - 1, fs],
-            recv_sem=y_recv.at[i, k - 1, fs],
+            src_ref=ref, dst_ref=ref, send_sem=y_send.at[i // cuts, k - 1, fs],
+            recv_sem=y_recv.at[i // cuts, k - 1, fs],
             device_id=at(rep, fs + inward, tp), device_id_type=MESH,
         )
 
     def y_copy(i, owner, k):
         ref = piece(i, owner, rep)
         return pltpu.make_async_remote_copy(
-            src_ref=ref, dst_ref=ref, send_sem=y_send.at[i, k - 1, owner],
-            recv_sem=y_recv.at[i, k - 1, owner],
+            src_ref=ref, dst_ref=ref, send_sem=y_send.at[i // cuts, k - 1, owner],
+            recv_sem=y_recv.at[i // cuts, k - 1, owner],
             device_id=at(lax.rem(rep + k, n_rep), fs, tp), device_id_type=MESH,
         )
 
@@ -215,7 +227,7 @@
 
         @pl.when(depth > low_depth(w))
         def _():
-            z_copy(i, fs, 1).start()
+            z_copy(i, fs, 1, True).start()
 
     def rest_end(i):
         for k in range(1, n_rep):
@@ -279,17 +291,14 @@
         if i + ahead < items:
             when_busy(lambda: own(i + ahead))
 
+    def y_share(w, owner, k, part_index):
+        return settled(
+            share_of(w, owner, part_index), y_send.at[w, k - 1, owner], y_recv.at[w, k - 1, owner]
+        )
+
     def arrived_one(w, owner):
-        for cut in range(cuts):
-            i = w * cuts + cut
-            for k in range(1, n_rep):
-                source = lax.rem(rep + n_rep - k, n_rep)
-                ref = piece(i, owner, source)
-                pltpu.make_async_remote_copy(
-                    src_ref=ref, dst_ref=ref, send_sem=y_send.at[i, k - 1, owner],
-                    recv_sem=y_recv.at[i, k - 1, owner],
-                    device_id=at(source, fs, tp), device_id_type=MESH,
-                ).wait_recv()
+        for k in range(1, n_rep):
+            y_share(w, owner, k, lax.rem(rep + n_rep - k, n_rep)).wait_recv()
 
     def arrived(w):
         def one(h, carry):
@@ -299,20 +308,23 @@
         lax.fori_loop(1, n_fs, one, 0)
 
     def sends_done():
+        def z_done(w, owner, send):
+            settled(share_of(w, owner, rep), send, z_recv.at[w * cuts, owner]).wait_send()
+
         def one(owner, carry):
             offset = inward * (owner - fs)
-            for i in range(items):
-                low = low_depth(i // cuts)
+            for w in range(6):
+                low = low_depth(w)
                 if n_fs > 1:
-                    passed = (offset == 0) | ((offset < 0) & (depth >= low))
-
-                    @pl.when(passed)
+                    outer = (offset < 0) & (depth >= low)
+
+                    @pl.when((offset == 0) | outer | ((offset > 0) & (depth > low)))
                     def _():
-                        z_copy(i, owner, 0).wait_send()
-
-                @pl.when((offset >= 0) & (depth > low))
-                def _():
-                    z_copy(i, owner, 1).wait_send()
+                        z_done(w, owner, z_send.at[w, owner])
+
+                    @pl.when((offset == 0) & (depth > low))
+                    def _():
+                        z_done(w, owner, out_send.at[w])
 
                 sent = (offset != 0) & (depth >= low)
                 if spread:
@@ -321,16 +333,16 @@
                 @pl.when(sent)
                 def _():
                     for k in range(1, n_rep):
-                        y_copy(i, owner, k).wait_send()
+                        y_share(w, owner, k, rep).wait_send()
 
             return carry
 
         lax.fori_loop(0, n_fs, one, 0)
 
         def rest():
-            for i in range(items):
+            for w in range(6):
                 for k in range(1, n_rep):
-                    rest_copy(i, k).wait_send()
+                    y_share(w, fs, k, lax.rem(rep + n_rep - k, n_rep)).wait_send()
 
         when_end(rest)
 
@@ -353,12 +365,12 @@
         ref = rows_all.at[s, chip, rows]
         target = other_chip(k) * 2 + core
         return tp_copy(
-            ref, ref, ag_sem.at[0, phase, s, k, c], ag_sem.at[1, phase, s, k, c], target
+            ref, ref, ag_sem.at[0, s, k - 1, c], ag_sem.at[1, s, k - 1, c], target
         )
 
     def pass_copy(phase, s, k):
         ref = rows_all.at[s, source_chip(k), mine]
-        return tp_copy(ref, ref, agf_sem.at[0, phase, s, k], agf_sem.at[1, phase, s, k], sibling)
+        return tp_copy(ref, ref, agf_sem.at[0, s, k], agf_sem.at[1, s, k], sibling)
 
     def gather_send(phase, s, c):
         for k in range(1, n_chip):
@@ -413,7 +425,7 @@
     def chip_copy(s, k, f):
         return tp_copy(
             to_chip.at[s, k - 1, f], from_chip.at[s, k - 1, f],
-            chip_sem.at[0, s, k, f], chip_sem.at[1, s, k, f], other_chip(k) * 2 + core,
+            chip_sem.at[0, s, k - 1, f], chip_sem.at[1, s, k - 1, f], other_chip(k) * 2 + core,
         )
 
     def product(s, p, f, left, w):
@@ -570,10 +582,7 @@
 
     def own_first():
         first_of(1)
-        if spread:
-            pl.when(depth != 1)(lambda: gather_rest(1, 1))
-        else:
-            gather_rest(1, 1)
+        gather_rest(1, 1)
         each_slot(reduce_end)
 
     def guest_lifts():
@@ -606,17 +615,17 @@
 
     def mom_copy(s, k):
         return tp_copy(
-            mom_own.at[s], mom_in.at[s, k - 1], mom_sem.at[0, s, k], mom_sem.at[1, s, k],
+            mom_own.at[s], mom_in.at[s, k - 1], mom_sem.at[0, s, k - 1], mom_sem.at[1, s, k - 1],
             lax.rem(tp + k, n_tp),
         )
 
     def values_of(s):
         gather_pass(1, s)
         gather_in(1, s)
-        each_pair(lambda p: u_pair(s, p))
         each_pair(lambda p: v_pair(s, p))
         for k in range(1, n_tp):
             mom_copy(s, k).start()
+        each_pair(lambda p: u_pair(s, p))
         gather_end(1, s)
 
     def mix_of(s):
@@ -652,7 +661,6 @@
 
     def guest_values():
         values_of(0)
-        gather_rest(1, 1)
 
     def mixer_in():
         row = lax.broadcasted_iota(jnp.int32, (SPAN, SPAN), 0)
@@ -691,7 +699,7 @@
 
     def bands_of(start, stop, run):
         def one(h, carry):
-            run(lax.rem(fs + h, n_fs))
+            run(nth_owner(h))
             return carry
 
         lax.fori_loop(start, stop, one, 0)
@@ -716,10 +724,11 @@
 
         def guest_in():
             mix_of(0)
-            arrived(MIX_DOWN)
+            bands_of(1, middle, lambda f: arrived_one(MIX_DOWN, f))
             span_of(0, 0, middle)
 
         def guest_rest():
+            bands_of(middle, n_fs, lambda f: arrived_one(MIX_DOWN, f))
             span_of(0, middle, n_fs)
             ship(0, middle)
 
@@ -753,24 +762,24 @@
     def gather_half(k, c):
         ref = rows_last.at[chip, c, core]
         target = other_chip(k) * 2 + core
-        return tp_copy(ref, ref, agl_sem.at[0, k, c], agl_sem.at[1, k, c], target)
+        return tp_copy(ref, ref, ag_sem.at[0, 1, k - 1, c], ag_sem.at[1, 1, k - 1, c], target)
 
     def pass_half(k, c):
         ref = rows_last.at[source_chip(k), c, core]
-        return tp_copy(ref, ref, agl_sem.at[2, k, c], agl_sem.at[3, k, c], sibling)
+        return tp_copy(ref, ref, agf_sem.at[0, c, k], agf_sem.at[1, c, k], sibling)
 
     def sib_half(p, f, c):
         rows = pl.ds(c * half, half)
         return tp_copy(
             to_sibling.at[1, p, f, rows], from_sibling.at[1, p, f, rows],
-            last_sem.at[0, p, f, c], last_sem.at[1, p, f, c], sibling,
+            sib_sem.at[0, c, p, f], sib_sem.at[1, c, p, f], sibling,
         )
 
     def chip_half(k, f, c):
         rows = pl.ds(c * half, half)
         return tp_copy(
             to_chip.at[1, k - 1, f, rows], from_chip.at[1, k - 1, f, rows],
-            last_sem.at[2, k, f, c], last_sem.at[3, k, f, c], other_chip(k) * 2 + core,
+            chip_sem.at[0, c, k - 1, f], chip_sem.at[1, c, k - 1, f], other_chip(k) * 2 + core,
         )
 
     normed = norm_rows(resid[1].astype(jnp.float32), gain_after[...])
@@ -815,6 +824,16 @@
     for c in range(HALVES):
         pass_half(0, c).wait_recv()
         last_rows(chip, c)
+
+    when_end(lambda: token_copy().wait_send())
+
+    def shipped():
+        for f in range(n_fs):
+            second_copy(f).wait_send()
+
+    when_mid(shipped)
+    sends_done()
+
     for c in range(HALVES):
         for k in range(1, n_chip):
             gather_half(k, c).wait_recv()
@@ -823,9 +842,9 @@
             pass_half(k, c).wait_recv()
             last_rows(other_chip(k), c)
             last_products(other_chip(k), c)
+        for k in range(1, n_chip):
+            last_joins(k, c)
         last_products(chip, c)
-        for k in range(1, n_chip):
-            last_joins(k, c)
     for f in range(n_fs):
         for c in range(HALVES):
             sib_half(chip, f, c).wait_recv()
@@ -851,14 +870,6 @@
         return carry
 
     lax.fori_loop(0, n_fs, last_sent, 0)
-    when_end(lambda: token_copy().wait_send())
-
-    def shipped():
-        for f in range(n_fs):
-            second_copy(f).wait_send()
-
-    when_mid(shipped)
-    sends_done()
 
 
 def body(
@@ -927,19 +938,18 @@
             pltpu.VMEM((128, SPAN), f32),
             pltpu.VMEM((2, block, width), bf16),
             dma((6,)),
-            dma((2, 6 * cuts, n_fs)),
+            dma((6, n_fs)),
+            dma((6,)),
             dma((6 * cuts, n_fs)),
-            dma((6 * cuts, spread_reps, n_fs)),
-            dma((6 * cuts, spread_reps, n_fs)),
-            dma((2, 2, 2, n_chip, HALVES)),
-            dma((2, 2, 2, n_chip)),
+            dma((6, spread_reps, n_fs)),
+            dma((6, spread_reps, n_fs)),
+            dma((2, 2, spread_chips, HALVES)),
+            dma((2, 2, n_chip)),
             dma((2, 2, n_chip, n_fs)),
-            dma((2, 2, n_chip, n_fs)),
-            dma((2, 2, n_tp)),
+            dma((2, 2, spread_chips, n_fs)),
+            dma((2, 2, max(n_tp - 1, 1))),
             dma((2,)),
             dma((2, n_fs)),
-            dma((4, n_chip, HALVES)),
-            dma((4, n_chip, n_fs, HALVES)),
         ],
         compiler_params=pltpu.CompilerParams(
             collective_id=0, has_side_effects=True, vmem_limit_bytes=60 * 1024 * 1024

time: 178 us -> 174 us (0.978)
  Pallas kernels: 176 us -> 173 us
    pallas_call x1, Pallas kernels: 176 us -> 173 us  [body(): pl.pallas_call(functools.partial(layer_kernel, n_rep, n_fs, n_tp), out_sh...]
where the time goes in v3:
time: 174 us
  Pallas kernels  173 us (99%)
    pallas_call x1, Pallas kernels, body(): pl.pallas_call(functools.partial(layer_kernel, n_rep, n_fs, n_tp), out_sh...  173 us

profile of v3, /device:TPU:16, one launch (start us, length us, event | category | flops | bytes accessed | tf_op | source)
XLA Modules:
  0.0 173.9 jit_solution(594050431447059977)
XLA Ops:
  0.0 173.1 %shard_map.136 = bf16[128,2048]{1,0:T(8,128)(2,1)S(1)} custom-call(bf16[128,2048]{1,0:T(8,128)(2,1)} %stream.1, f32[1,2048]{1,0:T(1,128)} %bitcast.5, f32[1,2048]{1,0:T(1,128)} %bitcast.6, f32[1,2048]{1,0:T(1,128)} %bitcast.7, f32[1,512]{1,0:T(1,128)} %bitcast.8, f32[1,512]{1,0:T(1,128)} %bitcast.9, bf16[4,128,128]{2,1,0:T(8,128)(2,1)} %spatial.1, ...), custom_call_target="tpu_custom_call" | custom-call | tf_op jit(solution)/shard_map/pallas_call | solution.py:908
  173.1 0.8 copy.16

commit v4 on v3

--- a/solution.py
+++ b/solution.py
@@ -163,11 +163,15 @@
     locals_ = [
         pltpu.make_async_copy(shards[w], whole(w, fs), local_sem.at[w]) for w in range(6)
     ]
-    for copy in locals_:
+    first_slot = jnp.minimum(depth, 1) if spread else 1
+    stream_in = pltpu.make_async_copy(stream, resid.at[first_slot], local_sem.at[6])
+    spatial_in = pltpu.make_async_copy(spatial, masked, local_sem.at[7])
+    for copy in [stream_in] + locals_ + [spatial_in]:
         copy.start()
 
     line_peers = jnp.minimum(fs, 1) + jnp.minimum(n_fs - 1 - fs, 1)
     pl.semaphore_wait(barrier, n_rep - 1 + n_tp - 1 + line_peers)
+    stream_in.wait()
 
     items = 6 * cuts
 
@@ -481,7 +485,7 @@
 
     def token_copy():
         return pltpu.make_async_remote_copy(
-            src_ref=stream, dst_ref=resid.at[0], send_sem=token_sem.at[0],
+            src_ref=resid.at[0], dst_ref=resid.at[0], send_sem=token_sem.at[0],
             recv_sem=token_sem.at[1], device_id=at(rep, fs + inward, tp), device_id_type=MESH,
         )
 
@@ -505,11 +509,11 @@
     def open_own():
         for i in range(ahead):
             own(i)
-        resid[1] = stream[...]
         gather_start(0, 1, gain_before)
         gather_rest(0, 1)
 
     when_busy(open_own)
+    spatial_in.wait()
     for i in range(near_by):
         near(i)
 
@@ -666,7 +670,7 @@
         row = lax.broadcasted_iota(jnp.int32, (SPAN, SPAN), 0)
         col = lax.broadcasted_iota(jnp.int32, (SPAN, SPAN), 1)
         for g in range(groups):
-            masked[g] = jnp.where(row >= col, spatial[g].astype(jnp.float32), 0.0).astype(
+            masked[g] = jnp.where(row >= col, masked[g].astype(jnp.float32), 0.0).astype(
                 jnp.bfloat16
             )
         square[...] = jnp.zeros_like(square)
@@ -908,7 +912,7 @@
     return pl.pallas_call(
         functools.partial(layer_kernel, n_rep, n_fs, n_tp),
         out_shape=pltpu.VMEM((block, width), bf16),
-        in_specs=[vmem] * 8 + [anywhere] * 6,
+        in_specs=[anywhere] + [vmem] * 5 + [anywhere, vmem] + [anywhere] * 6,
         out_specs=vmem,
         scratch_shapes=[
             pltpu.VMEM(
@@ -937,7 +941,7 @@
             pltpu.VMEM((2, max(n_tp - 1, 1), n_chip, 8, pair), f32),
             pltpu.VMEM((128, SPAN), f32),
             pltpu.VMEM((2, block, width), bf16),
-            dma((6,)),
+            dma((8,)),
             dma((6, n_fs)),
             dma((6,)),
             dma((6 * cuts, n_fs)),

time: 174 us -> 174 us (level)
  no operation moved by 1% of the time
where the time goes in v4:
time: 174 us
  Pallas kernels  173 us (99%)
    pallas_call x1, Pallas kernels, body(): pl.pallas_call(functools.partial(layer_kernel, n_rep, n_fs, n_tp), out_sh...  173 us

profile of v4, /device:TPU:16, one launch (start us, length us, event | category | flops | bytes accessed | tf_op | source)
XLA Modules:
  0.0 173.6 jit_solution(111135005037668747)
XLA Ops:
  0.0 172.8 %shard_map.136 = bf16[128,2048]{1,0:T(8,128)(2,1)S(1)} custom-call(bf16[128,2048]{1,0:T(8,128)(2,1)} %stream.1, f32[1,2048]{1,0:T(1,128)} %bitcast.5, f32[1,2048]{1,0:T(1,128)} %bitcast.6, f32[1,2048]{1,0:T(1,128)} %bitcast.7, f32[1,512]{1,0:T(1,128)} %bitcast.8, f32[1,512]{1,0:T(1,128)} %bitcast.9, bf16[4,128,128]{2,1,0:T(8,128)(2,1)} %spatial.1, ...), custom_call_target="tpu_custom_call" | custom-call | tf_op jit(solution)/shard_map/pallas_call | solution.py:912
  172.8 0.8 copy.16
